TPU v7x, 32 devices: a whole 2x2x4 slice. The times are simulated.
32 devices in a mesh: sp: 8 (over z, x), tp: 4 (over y, core).
Axes of the slice: x: 2, y: 2, z: 4, core: 2. Of those that a mesh axis runs over, the one named last changes fastest.
Arguments:
- queries: bfloat16 [4096, 512], P('sp', 'tp'), may hold values from -16 to 16
- key_heads: bfloat16 [4096, 512], P('sp', 'tp'), may hold values from -16 to 16
- value_heads: bfloat16 [4096, 512], P('sp', 'tp'), may hold values from -6 to 6
- head_gain: float32 [512], P('tp'), may hold values from 0.1 to 1.9
- residual: bfloat16 [4096, 2048], P(('sp', 'tp')), may hold values from -6 to 6
- out_weight: bfloat16 [512, 2048], replicated, may hold values from -0.25 to 0.25
- norm_gain: float32 [2048], replicated, may hold values from 0.1 to 1.9
- shared_gate: bfloat16 [2048, 512], replicated, may hold values from -0.125 to 0.125
- shared_up: bfloat16 [2048, 512], replicated, may hold values from -0.125 to 0.125
- shared_down: bfloat16 [512, 2048], replicated, may hold values from -0.25 to 0.25
- expert_gate: bfloat16 [64, 2048, 512], P(('sp', 'tp')), may hold values from -0.125 to 0.125
- expert_up: bfloat16 [64, 2048, 512], P(('sp', 'tp')), may hold values from -0.125 to 0.125
- expert_down: bfloat16 [64, 512, 2048], P(('sp', 'tp')), may hold values from -0.25 to 0.25
- routed_experts: int32 [4096, 4], P(('sp', 'tp')), may hold values from 0 to 63, all different within a row; in each aligned block of 128 rows (0 to 127, 128 to 255, ...) at most 12 rows name the same one
- route_weights: float32 [4096, 4], P(('sp', 'tp')), may hold values from 0.1 to 1.5
Outputs:
- layer_output: bfloat16 [4096, 2048], P(('sp', 'tp'))
Inputs may be any that keep to these rules, and one draw needn't show every extreme that they name: `routed_experts`: each row names 4 different experts. Within the rows of one device (128 consecutive rows, aligned) no expert is named more than 12 times, and in every draw some expert is named exactly 12 times in some device's rows.
All inputs are finite; a program needn't handle non-finite values.
Results may differ from a plain program's by a relative error of at most 0.014.
Values may be sent and summed in bfloat16 or wider, within the bound.
A program may use at most 128 MiB of HBM per device.

v0:
```python
import functools
import math

import jax
import jax.numpy as jnp
from jax import lax
from jax.experimental import pallas as pl
from jax.experimental.pallas import tpu as pltpu
from jax.sharding import PartitionSpec as P

HEAD_DIM = 64


EPSILON = 1e-06

COLUMNS = 2
TILE = 256
LOG2E = 1.4426950408889634
MESH = pl.DeviceIdType.MESH


def attention_kernel(rows, q_ref, kv_ref, gain_ref, out_ref, held, acc, carry, up_send, up_recv, side_send, side_recv):
    me = lax.axis_index("sp")
    row, col = me // COLUMNS, me % COLUMNS
    seq, width = q_ref.shape
    heads = width // HEAD_DIM
    tile = min(TILE, seq)
    tiles = seq // tile
    other = row * COLUMNS + (COLUMNS - 1 - col)

    barrier = pltpu.get_barrier_semaphore()

    @pl.when(row < rows - 1)
    def _():
        pl.semaphore_signal(barrier, inc=1, device_id={"sp": me + COLUMNS}, device_id_type=MESH)

    @pl.when(row > 0)
    def _():
        pl.semaphore_signal(barrier, inc=1, device_id={"sp": me - COLUMNS}, device_id_type=MESH)

    pl.semaphore_signal(barrier, inc=1, device_id={"sp": other}, device_id_type=MESH)
    inner = (row > 0) & (row < rows - 1)

    @pl.when(inner)
    def _():
        pl.semaphore_wait(barrier, 3)

    @pl.when(jnp.logical_not(inner))
    def _():
        pl.semaphore_wait(barrier, min(rows, 2))

    def up_copy(source, depth):
        place = (row - depth) * COLUMNS + col
        return pltpu.make_async_remote_copy(
            src_ref=source, dst_ref=held.at[place], send_sem=up_send.at[depth], recv_sem=up_recv.at[depth],
            device_id={"sp": me + COLUMNS}, device_id_type=MESH)

    def side_copy(source, depth):
        place = (row - depth) * COLUMNS + col
        return pltpu.make_async_remote_copy(
            src_ref=source, dst_ref=held.at[place], send_sem=side_send.at[depth], recv_sem=side_recv.at[depth],
            device_id={"sp": other}, device_id_type=MESH)

    @pl.when(row < rows - 1)
    def _():
        up_copy(kv_ref, 0).start()

    @pl.when(col == 0)
    def _():
        side_copy(kv_ref, 0).start()

    lane = lax.broadcasted_iota(jnp.int32, (1, width), 1) // HEAD_DIM
    key_row = lax.broadcasted_iota(jnp.int32, (tile, tile), 0)
    key_col = lax.broadcasted_iota(jnp.int32, (tile, tile), 1)
    later = (key_row > key_col).astype(jnp.bfloat16)
    scale = LOG2E / math.sqrt(HEAD_DIM)

    def one(source, key_tile, query_tile, head, diagonal):
        query_rows = slice(query_tile * tile, (query_tile + 1) * tile)
        key_rows = slice(key_tile * tile, (key_tile + 1) * tile)
        queries = jnp.where(lane == head, q_ref[query_rows, :], jnp.zeros((), q_ref.dtype))
        keys = source[key_rows, :width]
        values = source[key_rows, width:]
        scores = lax.dot_general(queries, keys, (((1,), (1,)), ((), ())), preferred_element_type=jnp.float32) * scale
        soft = jnp.log2(1.0 + jnp.exp2(-jnp.abs(scores)))
        take = jnp.minimum(scores, 0.0) - soft
        stay = take - scores
        if diagonal:
            stay = jnp.where(key_col < key_row, stay, 0.0)
        high = stay.astype(jnp.bfloat16)
        low = (stay - high.astype(jnp.float32)).astype(jnp.bfloat16)
        after = jnp.dot(high, later, preferred_element_type=jnp.float32) + jnp.dot(low, later, preferred_element_type=jnp.float32)
        before = carry[head, query_rows, :]
        weights = jnp.exp2(take + after + before)
        if diagonal:
            weights = jnp.where(key_col < key_row, weights, 0.0)
        part = jnp.dot(weights.astype(jnp.bfloat16), values, preferred_element_type=jnp.float32)
        acc[query_rows, :] += jnp.where(lane == head, part, 0.0)
        carry[head, query_rows, :] = before + (after[:, :1] + stay[:, :1])

    acc[...] = jnp.zeros_like(acc)
    carry[...] = jnp.zeros_like(carry)
    for key_tile in range(tiles - 1, -1, -1):
        for query_tile in range(key_tile, tiles):
            for head in range(heads):
                one(kv_ref, key_tile, query_tile, head, key_tile == query_tile)

    def receive(depth):
        place = (row - depth) * COLUMNS + col
        up_copy(held.at[place], depth - 1).wait_recv()

        @pl.when(row < rows - 1)
        def _():
            up_copy(held.at[place], depth).start()

        side_copy(held.at[place], depth).start()

    def step(index, unused):
        shard = me - 1 - index
        depth = row - shard // COLUMNS

        @pl.when(shard % COLUMNS != col)
        def _():
            @pl.when(depth + col <= row)
            def _():
                receive(depth + col)

            side_copy(held.at[shard], depth).wait_recv()

        source = held.at[shard]
        for key_tile in range(tiles - 1, -1, -1):
            for query_tile in range(tiles):
                for head in range(heads):
                    one(source, key_tile, query_tile, head, False)
        return unused

    lax.fori_loop(0, me, step, 0)

    def finish(depth, unused):
        @pl.when(row < rows - 1)
        def _():
            up_copy(kv_ref, depth).wait_send()

        @pl.when((col == 0) | (depth > 0))
        def _():
            side_copy(kv_ref, depth).wait_send()

        return unused

    lax.fori_loop(0, row + 1, finish, 0)

    mixed = acc[...]
    square = mixed * mixed
    inverse = jnp.zeros_like(mixed)
    for head in range(heads):
        mean = jnp.sum(jnp.where(lane == head, square, 0.0), axis=1, keepdims=True) * (1.0 / HEAD_DIM)
        inverse = jnp.where(lane == head, lax.rsqrt(mean + EPSILON), inverse)
    out_ref[...] = (mixed * inverse * gain_ref[...]).astype(out_ref.dtype)


def attention(queries, key_heads, value_heads, head_gain):
    seq, width = queries.shape
    shards = lax.axis_size("sp")
    rows = shards // COLUMNS
    heads = width // HEAD_DIM
    both = jnp.concatenate([key_heads, value_heads], axis=1)
    vmem = pl.BlockSpec(memory_space=pltpu.VMEM)
    return pl.pallas_call(
        functools.partial(attention_kernel, rows),
        out_shape=jax.ShapeDtypeStruct((seq, width), jnp.bfloat16),
        in_specs=[vmem] * 3,
        out_specs=vmem,
        scratch_shapes=[
            pltpu.VMEM((shards, seq, 2 * width), jnp.bfloat16),
            pltpu.VMEM((seq, width), jnp.float32),
            pltpu.VMEM((heads, seq, 1), jnp.float32),
            pltpu.SemaphoreType.DMA((rows,)),
            pltpu.SemaphoreType.DMA((rows,)),
            pltpu.SemaphoreType.DMA((rows,)),
            pltpu.SemaphoreType.DMA((rows,)),
        ],
        compiler_params=pltpu.CompilerParams(collective_id=0, has_side_effects=True),
        name="attention",
    )(queries, both, head_gain.reshape(1, width))


def round_up(value, unit):
    return (value + unit - 1) // unit * unit


def routed_sum(expert_input, expert_gate, expert_up, expert_down, routed_experts, route_weights):
    row_count, pick_count = routed_experts.shape
    local_experts = expert_gate.shape[0]
    model_width = expert_input.shape[1]
    device_count = lax.axis_size("sp") * lax.axis_size("tp")
    expert_count = local_experts * device_count
    capacity = max(2, 3 * row_count * pick_count // (2 * expert_count))
    span = round_up(local_experts * capacity, 8)
    flat_experts = routed_experts.reshape(-1)
    expert_table = (
        flat_experts[:, None] == jnp.arange(expert_count, dtype=jnp.int32)[None, :]
    ).astype(jnp.bfloat16)
    pick_row = lax.broadcasted_iota(jnp.int32, (flat_experts.shape[0],) * 2, 0)
    pick_col = lax.broadcasted_iota(jnp.int32, (flat_experts.shape[0],) * 2, 1)
    earlier = (pick_col < pick_row).astype(jnp.bfloat16)
    counts = jnp.dot(earlier, expert_table, preferred_element_type=jnp.float32)
    ranking = jnp.sum(counts * expert_table.astype(jnp.float32), axis=1).astype(jnp.int32)
    slot_index = (flat_experts // local_experts) * span + (flat_experts % local_experts) * capacity + ranking
    match = (
        slot_index.reshape(row_count, pick_count)[:, :, None]
        == jnp.arange(device_count * span, dtype=jnp.int32)[None, None, :]
    )
    token_place = jnp.sum(match.astype(jnp.float32), axis=1).astype(jnp.bfloat16)
    outgoing = jnp.einsum(
        "rs,rd->sd", token_place, expert_input, preferred_element_type=jnp.float32
    ).astype(jnp.bfloat16)
    outgoing = outgoing.reshape(device_count, span, model_width)
    arrived = lax.all_to_all(outgoing, ("sp", "tp"), split_axis=0, concat_axis=0, tiled=True)
    places = lax.broadcasted_iota(jnp.int32, (1, span, 1), 1)
    result = jnp.zeros(arrived.shape, jnp.bfloat16)
    for expert in range(local_experts):
        first = expert * capacity // 8 * 8
        last = round_up((expert + 1) * capacity, 8)
        grouped = arrived[:, first:last].reshape(-1, model_width)
        gate_part = jnp.dot(grouped, expert_gate[expert], preferred_element_type=jnp.float32)
        up_part = jnp.dot(grouped, expert_up[expert], preferred_element_type=jnp.float32)
        hidden = (jax.nn.silu(gate_part) * up_part).astype(jnp.bfloat16)
        down = jnp.dot(hidden, expert_down[expert], preferred_element_type=jnp.float32).astype(jnp.bfloat16)
        down = jnp.pad(down.reshape(device_count, last - first, model_width), ((0, 0), (first, span - last), (0, 0)))
        mine = (places >= expert * capacity) & (places < (expert + 1) * capacity)
        result = jnp.where(mine, down, result)
    returned = lax.all_to_all(result, ("sp", "tp"), split_axis=0, concat_axis=0, tiled=True)
    returned = returned.reshape(-1, model_width)
    token_weight = jnp.sum(jnp.where(match, route_weights[:, :, None], 0.0), axis=1)
    high = token_weight.astype(jnp.bfloat16)
    low = (token_weight - high.astype(jnp.float32)).astype(jnp.bfloat16)
    return jnp.dot(high, returned, preferred_element_type=jnp.float32) + jnp.dot(
        low, returned, preferred_element_type=jnp.float32
    )


def body(
    queries,
    key_heads,
    value_heads,
    head_gain,
    residual,
    out_weight,
    norm_gain,
    shared_gate,
    shared_up,
    shared_down,
    expert_gate,
    expert_up,
    expert_down,
    routed_experts,
    route_weights,
):
    head_output = attention(queries, key_heads, value_heads, head_gain)
    token_heads = lax.all_to_all(head_output, "tp", split_axis=0, concat_axis=1, tiled=True)
    branch = jnp.dot(token_heads, out_weight, preferred_element_type=jnp.float32)
    stream = (residual.astype(jnp.float32) + branch).astype(jnp.bfloat16)
    stream_wide = stream.astype(jnp.float32)
    inverse = lax.rsqrt(jnp.mean(stream_wide * stream_wide, axis=1, keepdims=True) + EPSILON)
    expert_input = (stream_wide * inverse * norm_gain).astype(jnp.bfloat16)
    shared_hidden = (
        jax.nn.silu(jnp.dot(expert_input, shared_gate, preferred_element_type=jnp.float32))
        * jnp.dot(expert_input, shared_up, preferred_element_type=jnp.float32)
    ).astype(jnp.bfloat16)
    shared_term = jnp.dot(shared_hidden, shared_down, preferred_element_type=jnp.float32)
    routed = routed_sum(
        expert_input, expert_gate, expert_up, expert_down, routed_experts, route_weights
    )
    return (stream_wide + shared_term + routed).astype(jnp.bfloat16)


def solution(mesh):
    return jax.shard_map(
        body,
        mesh=mesh,
        in_specs=(
            P("sp", "tp"),
            P("sp", "tp"),
            P("sp", "tp"),
            P("tp"),
            P(("sp", "tp"), None),
            P(),
            P(),
            P(),
            P(),
            P(),
            P(("sp", "tp"), None, None),
            P(("sp", "tp"), None, None),
            P(("sp", "tp"), None, None),
            P(("sp", "tp"), None),
            P(("sp", "tp"), None),
        ),
        out_specs=P(("sp", "tp"), None),
        check_vma=False,
    )
```

profile of v0, /device:TPU:0, one launch (start us, length us, event | category | flops | bytes accessed | tf_op | source)
XLA Modules:
  0.0 245.4 jit_solution(10402263451006479374)
XLA Ops:
  0.0 1.8 pad_maximum_fusion.kv_ref
  1.9 10.6 %attention.1 = bf16[512,128]{1,0:T(8,128)(2,1)} custom-call(bf16[512,128]{1,0:T(8,128)(2,1)} %q_ref.1, bf16[512,256]{1,0:T(8,128)(2,1)} %pad_maximum_fusion.kv_ref, f32[1,128]{1,0:T(1,128)} %bitcast.62), custom_call_target="tpu_custom_call" | custom-call | tf_op jit(solution)/shard_map/attention/pallas_call | solution.py:168
  12.5 1.7 copy.38
  14.2 3.3 %all-to-all-start = ((bf16[4,128,128]{1,2,0:T(8,128)(2,1)}), bf16[4,128,128]{1,2,0:T(8,128)(2,1)S(1)}, u32[]{:S(2)}, u32[]{:S(2)}) async-start(bf16[4,128,128]{1,2,0:T(8,128)(2,1)} %copy.38), calls=%async_computation | async-start | bytes 262144 | tf_op jit(solution)/shard_map/all_to_all | solution.py:260
  17.5 0.8 copy.39
  18.3 0.1 eq.30
  18.4 0.3 fusion.33
  18.7 0.1 convert_element_type.75
  18.8 0.1 copy.40
  18.9 0.0 copy-done.7
  18.9 0.0 copy-start.6
  18.9 1.0 select_reduce_fusion
  20.0 2.1 all-to-all-done
  22.1 0.6 copy-done.5
  22.7 1.7 multiply_reduce_fusion
  24.4 2.8 %convolution_convert_fusion = bf16[768,2048]{1,0:T(8,128)(2,1)} fusion(bf16[128,768]{1,0:T(8,128)(2,1)S(1)} %copy-done.4, f32[128,2048]{1,0:T(8,128)S(1)} %get-tuple-element.10, f32[2048]{0:T(1024)S(1)} %copy-done.6, f32[128]{0:T(128)S(1)} %add_rsqrt_fusion), kind=kOutput, calls=%fused_computation | convolution fusion | flops 405012480 | bytes 4399616 | tf_op jit(solution)/shard_map/rs,rd->sd/dot_general | solution.py:214
  27.2 37.5 %all-to-all-start.1 = ((bf16[32,24,2048]{2,1,0:T(8,128)(2,1)}), bf16[32,24,2048]{2,1,0:T(8,128)(2,1)}, u32[]{:S(2)}, u32[]{:S(2)}) async-start(bf16[32,24,2048]{2,1,0:T(8,128)(2,1)} %bitcast.53), calls=%async_computation.1 | async-start | bytes 6291456 | tf_op jit(solution)/shard_map/all_to_all | solution.py:218
  64.7 0.5 compare_and_fusion
  65.2 70.9 %all-to-all-done.1 = bf16[32,24,2048]{2,1,0:T(8,128)(2,1)} async-done(((bf16[32,24,2048]{2,1,0:T(8,128)(2,1)}), bf16[32,24,2048]{2,1,0:T(8,128)(2,1)}, u32[]{:S(2)}, u32[]{:S(2)}) %all-to-all-start.1) | async-done | bytes 3145760 | tf_op jit(solution)/shard_map/all_to_all | solution.py:218
  136.1 2.9 %fusion.62 = (bf16[32,16,2048]{2,1,0:T(8,128)(2,1)S(1)}, bf16[32,16,2048]{2,1,0:T(8,128)(2,1)S(1)}) fusion(bf16[32,24,2048]{2,1,0:T(8,128)(2,1)} %all-to-all-done.1), kind=kLoop, calls=%fused_computation.77 | loop fusion | bytes 8388608 | tf_op jit(solution)/shard_map/slice | solution.py:224
  139.1 0.5 copy-done.9
  139.6 2.3 fusion.7
  141.9 2.2 fusion.12
  144.1 7.0 %convolution_convert_fusion.1 = bf16[512,2048]{1,0:T(8,128)(2,1)} fusion(bf16[2,512,2048]{2,1,0:T(8,128)(2,1)} %param.27, bf16[512,2048]{1,0:T(8,128)(2,1)} %bitcast.59, bf16[2,2048,512]{2,1,0:T(8,128)(2,1)} %param.26, f32[512,512]{1,0:T(8,128)} %fusion.7), kind=kOutput, calls=%fused_computation.2 | convolution fusion | flops 2150105088 | bytes 9437184 | tf_op jit(solution)/shard_map/dot_general | solution.py:228
  151.0 7.0 %convolution_convert_fusion.2 = bf16[512,2048]{1,0:T(8,128)(2,1)} fusion(bf16[2,512,2048]{2,1,0:T(8,128)(2,1)} %param.27, bf16[512,2048]{1,0:T(8,128)(2,1)} %bitcast.56, bf16[2,2048,512]{2,1,0:T(8,128)(2,1)} %param.26, f32[512,512]{1,0:T(8,128)} %fusion.12), kind=kOutput, calls=%fused_computation.3 | convolution fusion | flops 2150105088 | bytes 9437184 | tf_op jit(solution)/shard_map/dot_general | solution.py:228
  158.0 5.2 %select_select_fusion = bf16[32,24,2048]{2,1,0:T(8,128)(2,1)} fusion(bf16[32,16,2048]{2,1,0:T(8,128)(2,1)} %bitcast.54, bf16[32,16,2048]{2,1,0:T(8,128)(2,1)} %bitcast.57, pred[24]{0:T(512)(128)(4,1)} %get-tuple-element.12, pred[24]{0:T(512)(128)(4,1)S(1)} %get-tuple-element.11), kind=kLoop, calls=%fused_computation.1 | loop fusion | flops 3145728 | bytes 7340080 | tf_op jit(solution)/shard_map/jit(_where)/select_n | solution.py:231
  163.2 4.7 %all-to-all-start.2 = ((bf16[32,24,2048]{2,1,0:T(8,128)(2,1)}), bf16[32,24,2048]{2,1,0:T(8,128)(2,1)}, u32[]{:S(2)}, u32[]{:S(2)}) async-start(bf16[32,24,2048]{2,1,0:T(8,128)(2,1)} %select_select_fusion), calls=%async_computation.2 | async-start | bytes 6291456 | tf_op jit(solution)/shard_map/all_to_all | solution.py:232
  167.9 2.8 %fusion.61 = f32[128,512]{1,0:T(8,128)} fusion(bf16[2048,512]{1,0:T(8,128)(2,1)} %param.22, f32[128,2048]{1,0:T(8,128)S(1)} %get-tuple-element.10, f32[2048]{0:T(1024)S(1)} %copy-done.6, f32[128]{0:T(128)S(1)} %add_rsqrt_fusion), kind=kOutput, calls=%fused_computation.76 | convolution fusion | flops 269221888 | bytes 3416576 | tf_op jit(solution)/shard_map/dot_general | solution.py:267
  170.6 4.2 %convolution_add_fusion.1 = f32[128,2048]{1,0:T(8,128)} fusion(f32[128,2048]{1,0:T(8,128)S(1)} %get-tuple-element.10, bf16[512,2048]{1,0:T(8,128)(2,1)} %param.24, bf16[2048,512]{1,0:T(8,128)(2,1)} %param.23, f32[128,512]{1,0:T(8,128)} %fusion.61, f32[2048]{0:T(1024)S(1)} %copy-done.6, f32[128]{0:T(128)S(1)} %add_rsqrt_fusion), kind=kOutput, calls=%fused_computation.6 | convolution fusion | flops 538312704 | bytes 6562304 | tf_op jit(solution)/shard_map/dot_general | solution.py:270
  174.8 64.6 %all-to-all-done.2 = bf16[32,24,2048]{2,1,0:T(8,128)(2,1)} async-done(((bf16[32,24,2048]{2,1,0:T(8,128)(2,1)}), bf16[32,24,2048]{2,1,0:T(8,128)(2,1)}, u32[]{:S(2)}, u32[]{:S(2)}) %all-to-all-start.2) | async-done | bytes 3145760 | tf_op jit(solution)/shard_map/all_to_all | solution.py:232
  239.5 2.6 %fusion.49 = f32[128,2048]{1,0:T(8,128)S(1)} fusion(bf16[768,2048]{1,0:T(8,128)(2,1)} %bitcast.15, f32[128,768]{1,0:T(8,128)S(1)} %get-tuple-element.5), kind=kOutput, calls=%fused_computation.55 | convolution fusion | flops 402751488 | bytes 4587520 | tf_op jit(solution)/shard_map/dot_general | solution.py:237
  242.0 3.3 %fusion.3 = bf16[128,2048]{1,0:T(8,128)(2,1)} fusion(f32[128,2048]{1,0:T(8,128)S(1)} %copy-done.1, f32[128,2048]{1,0:T(8,128)S(1)} %fusion.49, bf16[768,2048]{1,0:T(8,128)(2,1)} %bitcast.15, f32[128,768]{1,0:T(8,128)S(1)} %get-tuple-element.5), kind=kOutput, calls=%fused_computation.10 | convolution fusion | flops 403832832 | bytes 6160384 | tf_op jit(solution)/shard_map/dot_general | solution.py:237
  (19 shorter events, 0.1 us)
Async XLA Ops:
  0.0 22.7 %copy-start = (bf16[512,2048]{1,0:T(8,128)(2,1)S(1)}, bf16[512,2048]{1,0:T(8,128)(2,1)}, u32[]{:S(2)}) copy-start(bf16[512,2048]{1,0:T(8,128)(2,1)} %param.20) | copy-start | bytes 6291460
  0.0 18.9 %copy-start.7 = (s32[128,4]{0,1:T(4,128)S(1)}, s32[128,4]{0,1:T(4,128)}, u32[]{:S(2)}) copy-start(s32[128,4]{0,1:T(4,128)} %param.28) | copy-start | bytes 6148
  0.0 18.9 %copy-start.8 = (f32[128,4]{0,1:T(4,128)S(1)}, f32[128,4]{0,1:T(4,128)}, u32[]{:S(2)}) copy-start(f32[128,4]{0,1:T(4,128)} %param.29) | copy-start | bytes 6148
  14.2 7.9 %all-to-all-start = ((bf16[4,128,128]{1,2,0:T(8,128)(2,1)}), bf16[4,128,128]{1,2,0:T(8,128)(2,1)S(1)}, u32[]{:S(2)}, u32[]{:S(2)}) async-start(bf16[4,128,128]{1,2,0:T(8,128)(2,1)} %copy.38), calls=%async_computation | async-start | bytes 262144 | tf_op jit(solution)/shard_map/all_to_all | solution.py:260
  18.9 5.5 %copy-start.6 = (f32[2048]{0:T(1024)S(1)}, f32[2048]{0:T(1024)}, u32[]{:S(2)}) copy-start(f32[2048]{0:T(1024)} %param.21) | copy-start | bytes 24580
  22.1 0.7 copy-start.5
  22.7 1.7 copy-start.4
  27.2 109.0 %all-to-all-start.1 = ((bf16[32,24,2048]{2,1,0:T(8,128)(2,1)}), bf16[32,24,2048]{2,1,0:T(8,128)(2,1)}, u32[]{:S(2)}, u32[]{:S(2)}) async-start(bf16[32,24,2048]{2,1,0:T(8,128)(2,1)} %bitcast.53), calls=%async_computation.1 | async-start | bytes 6291456 | tf_op jit(solution)/shard_map/all_to_all | solution.py:218
  136.1 3.5 %copy-start.9 = (bf16[2,2048,512]{2,1,0:T(8,128)(2,1)S(1)}, bf16[2,2048,512]{2,1,0:T(8,128)(2,1)}, u32[]{:S(2)}) copy-start(bf16[2,2048,512]{2,1,0:T(8,128)(2,1)} %param.25) | copy-start | bytes 12582916
  139.0 2.8 %copy-start.3 = (bf16[32,16,2048]{2,1,0:T(8,128)(2,1)}, bf16[32,16,2048]{2,1,0:T(8,128)(2,1)S(1)}, u32[]{:S(2)}) copy-start(bf16[32,16,2048]{2,1,0:T(8,128)(2,1)S(1)} %get-tuple-element.8) | copy-start | bytes 6291460
  139.0 2.8 %copy-start.2 = (bf16[32,16,2048]{2,1,0:T(8,128)(2,1)}, bf16[32,16,2048]{2,1,0:T(8,128)(2,1)S(1)}, u32[]{:S(2)}) copy-start(bf16[32,16,2048]{2,1,0:T(8,128)(2,1)S(1)} %get-tuple-element.7) | copy-start | bytes 6291460
  163.2 76.3 %all-to-all-start.2 = ((bf16[32,24,2048]{2,1,0:T(8,128)(2,1)}), bf16[32,24,2048]{2,1,0:T(8,128)(2,1)}, u32[]{:S(2)}, u32[]{:S(2)}) async-start(bf16[32,24,2048]{2,1,0:T(8,128)(2,1)} %select_select_fusion), calls=%async_computation.2 | async-start | bytes 6291456 | tf_op jit(solution)/shard_map/all_to_all | solution.py:232
  239.5 2.6 %copy-start.1 = (f32[128,2048]{1,0:T(8,128)S(1)}, f32[128,2048]{1,0:T(8,128)}, u32[]{:S(2)}) copy-start(f32[128,2048]{1,0:T(8,128)} %convolution_add_fusion.1) | copy-start | bytes 3145732
where the time goes:
time: 246 us; the launch traced here: 245 us
  waiting for transfers between devices  138 us (56%)
  starting transfers between devices  45.5 us (18%)
  matrix products  36 us (15%)
  Pallas kernels  10.6 us (4%)
  other arithmetic  8.62 us (4%)
  local copies, waits for them, and re-layouts  6.83 us (3%)
    all_to_all x1, waiting for transfers between devices, routed_sum(): lax.all_to_all(outgoing, ('sp', 'tp'), split_axis=0, concat_axis=0, tiled...  70.9 us
    all_to_all x1, waiting for transfers between devices, routed_sum(): lax.all_to_all(result, ('sp', 'tp'), split_axis=0, concat_axis=0, tiled=T...  64.6 us
    all_to_all x1, starting transfers between devices, routed_sum(): lax.all_to_all(outgoing, ('sp', 'tp'), split_axis=0, concat_axis=0, tiled...  37.5 us
    dot_general x2, matrix products, routed_sum(): jnp.dot(hidden, expert_down[expert], preferred_element_type=jnp.float32)  13.9 us
    pallas_call x1, Pallas kernels, attention(): pl.pallas_call(functools.partial(attention_kernel, rows), out_shape=jax.S...  10.6 us
    select_n x1, other arithmetic, routed_sum(): result = jnp.where(mine, down, result)  5.17 us
  transfers between devices with their start and end apart: 3, of which 3 were waited for; matrix products, arithmetic and copies ran while one was open for 4% of the time, Pallas kernels for 0%

commit v1 on v0

--- a/solution.py
+++ b/solution.py
@@ -19,7 +19,7 @@
 MESH = pl.DeviceIdType.MESH
 
 
-def attention_kernel(rows, q_ref, kv_ref, gain_ref, out_ref, held, acc, carry, up_send, up_recv, side_send, side_recv):
+def attention_kernel(rows, q_ref, kv_ref, gain_ref, out_ref, held, masked, acc, carry, up_send, up_recv, side_send, side_recv):
     me = lax.axis_index("sp")
     row, col = me // COLUMNS, me % COLUMNS
     seq, width = q_ref.shape
@@ -75,35 +75,41 @@
     later = (key_row > key_col).astype(jnp.bfloat16)
     scale = LOG2E / math.sqrt(HEAD_DIM)
 
-    def one(source, key_tile, query_tile, head, diagonal):
-        query_rows = slice(query_tile * tile, (query_tile + 1) * tile)
+    for head in range(heads):
+        for query_tile in range(tiles):
+            source_rows = slice(query_tile * tile, (query_tile + 1) * tile)
+            stacked_rows = slice((query_tile * heads + head) * tile, (query_tile * heads + head + 1) * tile)
+            masked[stacked_rows, :] = jnp.where(lane == head, q_ref[source_rows, :], jnp.zeros((), q_ref.dtype))
+
+    def span(source, key_tile, first, last, diagonal):
+        stacked_rows = slice(first * heads * tile, last * heads * tile)
         key_rows = slice(key_tile * tile, (key_tile + 1) * tile)
-        queries = jnp.where(lane == head, q_ref[query_rows, :], jnp.zeros((), q_ref.dtype))
         keys = source[key_rows, :width]
         values = source[key_rows, width:]
-        scores = lax.dot_general(queries, keys, (((1,), (1,)), ((), ())), preferred_element_type=jnp.float32) * scale
+        scores = lax.dot_general(masked[stacked_rows, :], keys, (((1,), (1,)), ((), ())), preferred_element_type=jnp.float32) * scale
         soft = jnp.log2(1.0 + jnp.exp2(-jnp.abs(scores)))
         take = jnp.minimum(scores, 0.0) - soft
         stay = take - scores
         if diagonal:
-            stay = jnp.where(key_col < key_row, stay, 0.0)
+            query_place = jnp.concatenate([key_row] * ((last - first) * heads), axis=0)
+            key_place = jnp.concatenate([key_col] * ((last - first) * heads), axis=0)
+            stay = jnp.where(key_place < query_place, stay, 0.0)
         high = stay.astype(jnp.bfloat16)
         low = (stay - high.astype(jnp.float32)).astype(jnp.bfloat16)
         after = jnp.dot(high, later, preferred_element_type=jnp.float32) + jnp.dot(low, later, preferred_element_type=jnp.float32)
-        before = carry[head, query_rows, :]
+        before = carry[stacked_rows, :]
         weights = jnp.exp2(take + after + before)
         if diagonal:
-            weights = jnp.where(key_col < key_row, weights, 0.0)
-        part = jnp.dot(weights.astype(jnp.bfloat16), values, preferred_element_type=jnp.float32)
-        acc[query_rows, :] += jnp.where(lane == head, part, 0.0)
-        carry[head, query_rows, :] = before + (after[:, :1] + stay[:, :1])
+            weights = jnp.where(key_place < query_place, weights, 0.0)
+        acc[stacked_rows, :] += jnp.dot(weights.astype(jnp.bfloat16), values, preferred_element_type=jnp.float32)
+        carry[stacked_rows, :] = before + (after[:, :1] + stay[:, :1])
 
     acc[...] = jnp.zeros_like(acc)
     carry[...] = jnp.zeros_like(carry)
     for key_tile in range(tiles - 1, -1, -1):
-        for query_tile in range(key_tile, tiles):
-            for head in range(heads):
-                one(kv_ref, key_tile, query_tile, head, key_tile == query_tile)
+        span(kv_ref, key_tile, key_tile, key_tile + 1, True)
+        if key_tile + 1 < tiles:
+            span(kv_ref, key_tile, key_tile + 1, tiles, False)
 
     def receive(depth):
         place = (row - depth) * COLUMNS + col
@@ -129,9 +135,7 @@
 
         source = held.at[shard]
         for key_tile in range(tiles - 1, -1, -1):
-            for query_tile in range(tiles):
-                for head in range(heads):
-                    one(source, key_tile, query_tile, head, False)
+            span(source, key_tile, 0, tiles, False)
         return unused
 
     lax.fori_loop(0, me, step, 0)
@@ -149,13 +153,16 @@
 
     lax.fori_loop(0, row + 1, finish, 0)
 
-    mixed = acc[...]
-    square = mixed * mixed
-    inverse = jnp.zeros_like(mixed)
-    for head in range(heads):
-        mean = jnp.sum(jnp.where(lane == head, square, 0.0), axis=1, keepdims=True) * (1.0 / HEAD_DIM)
-        inverse = jnp.where(lane == head, lax.rsqrt(mean + EPSILON), inverse)
-    out_ref[...] = (mixed * inverse * gain_ref[...]).astype(out_ref.dtype)
+    for query_tile in range(tiles):
+        mixed = jnp.zeros((tile, width), jnp.float32)
+        inverse = jnp.zeros((tile, width), jnp.float32)
+        for head in range(heads):
+            place = (query_tile * heads + head) * tile
+            own = jnp.where(lane == head, acc[place : place + tile, :], 0.0)
+            mean = jnp.sum(own * own, axis=1, keepdims=True) * (1.0 / HEAD_DIM)
+            mixed = mixed + own
+            inverse = jnp.where(lane == head, lax.rsqrt(mean + EPSILON), inverse)
+        out_ref[query_tile * tile : (query_tile + 1) * tile, :] = (mixed * inverse * gain_ref[...]).astype(out_ref.dtype)
 
 
 def attention(queries, key_heads, value_heads, head_gain):
@@ -172,8 +179,9 @@
         out_specs=vmem,
         scratch_shapes=[
             pltpu.VMEM((shards, seq, 2 * width), jnp.bfloat16),
-            pltpu.VMEM((seq, width), jnp.float32),
-            pltpu.VMEM((heads, seq, 1), jnp.float32),
+            pltpu.VMEM((heads * seq, width), jnp.bfloat16),
+            pltpu.VMEM((heads * seq, width), jnp.float32),
+            pltpu.VMEM((heads * seq, 1), jnp.float32),
             pltpu.SemaphoreType.DMA((rows,)),
             pltpu.SemaphoreType.DMA((rows,)),
             pltpu.SemaphoreType.DMA((rows,)),
@@ -234,9 +242,8 @@
     token_weight = jnp.sum(jnp.where(match, route_weights[:, :, None], 0.0), axis=1)
     high = token_weight.astype(jnp.bfloat16)
     low = (token_weight - high.astype(jnp.float32)).astype(jnp.bfloat16)
-    return jnp.dot(high, returned, preferred_element_type=jnp.float32) + jnp.dot(
-        low, returned, preferred_element_type=jnp.float32
-    )
+    both = jnp.dot(jnp.concatenate([high, low], axis=0), returned, preferred_element_type=jnp.float32)
+    return both[:row_count] + both[row_count:]
 
 
 def body(

time: 246 us -> 242 us (0.984)
  starting transfers between devices: 45.5 us -> 39 us
  waiting for transfers between devices: 138 us -> 142 us
    all_to_all x1, starting transfers between devices: 37.5 us -> 30.9 us  [routed_sum(): lax.all_to_all(outgoing, ('sp', 'tp'), split_axis=0, concat_axis=0, tiled...]
    all_to_all x1, waiting for transfers between devices: 64.6 us -> 68.7 us  [routed_sum(): lax.all_to_all(result, ('sp', 'tp'), split_axis=0, concat_axis=0, tiled=T...]
    dot_general x2 -> x1, matrix products: 5.89 us -> 4.43 us  [routed_sum(): jnp.dot(jnp.concatenate([high, low], axis=0), returned, preferred_element...]
  transfers between devices with their start and end apart: 3 -> 3, of which waited for: 3 -> 3; matrix products, arithmetic and copies ran while one was open for 4% -> 2% of each run, Pallas kernels for 0% -> 0%
where the time goes in v1:
time: 242 us
  waiting for transfers between devices  142 us (59%)
  starting transfers between devices  39 us (16%)
  matrix products  34.2 us (14%)
  Pallas kernels  10.7 us (4%)
  other arithmetic  9.39 us (4%)
  local copies, waits for them, and re-layouts  6.83 us (3%)
    all_to_all x1, waiting for transfers between devices, routed_sum(): lax.all_to_all(outgoing, ('sp', 'tp'), split_axis=0, concat_axis=0, tiled...  70.9 us
    all_to_all x1, waiting for transfers between devices, routed_sum(): lax.all_to_all(result, ('sp', 'tp'), split_axis=0, concat_axis=0, tiled=T...  68.7 us
    all_to_all x1, starting transfers between devices, routed_sum(): lax.all_to_all(outgoing, ('sp', 'tp'), split_axis=0, concat_axis=0, tiled...  30.9 us
    dot_general x2, matrix products, routed_sum(): jnp.dot(hidden, expert_down[expert], preferred_element_type=jnp.float32)  13.9 us
    pallas_call x1, Pallas kernels, attention(): pl.pallas_call(functools.partial(attention_kernel, rows), out_shape=jax.S...  10.7 us
    select_n x1, other arithmetic, routed_sum(): result = jnp.where(mine, down, result)  5.17 us
  transfers between devices with their start and end apart: 3, of which 3 were waited for; matrix products, arithmetic and copies ran while one was open for 2% of the time, Pallas kernels for 0%

profile of v1, /device:TPU:0, one launch (start us, length us, event | category | flops | bytes accessed | tf_op | source)
XLA Modules:
  0.0 241.9 jit_solution(2011154182114934235)
XLA Ops:
  0.0 1.8 pad_maximum_fusion.kv_ref
  1.9 10.7 %attention.1 = bf16[512,128]{1,0:T(8,128)(2,1)} custom-call(bf16[512,128]{1,0:T(8,128)(2,1)} %q_ref.1, bf16[512,256]{1,0:T(8,128)(2,1)} %pad_maximum_fusion.kv_ref, f32[1,128]{1,0:T(1,128)} %bitcast.61), custom_call_target="tpu_custom_call" | custom-call | tf_op jit(solution)/shard_map/attention/pallas_call | solution.py:175
  12.5 1.7 copy.38
  14.2 3.3 %all-to-all-start = ((bf16[4,128,128]{1,2,0:T(8,128)(2,1)}), bf16[4,128,128]{1,2,0:T(8,128)(2,1)S(1)}, u32[]{:S(2)}, u32[]{:S(2)}) async-start(bf16[4,128,128]{1,2,0:T(8,128)(2,1)} %copy.38), calls=%async_computation | async-start | bytes 262144 | tf_op jit(solution)/shard_map/all_to_all | solution.py:267
  17.5 0.8 copy.39
  18.3 0.1 eq.30
  18.4 0.3 fusion.33
  18.7 0.1 convert_element_type.75
  18.8 0.1 copy.40
  18.9 0.0 copy-done.7
  18.9 0.0 copy-start.5
  18.9 1.0 select_reduce_fusion
  20.0 2.1 all-to-all-done
  22.1 0.6 copy-done.4
  22.7 1.7 multiply_reduce_fusion
  24.5 2.8 %convolution_convert_fusion = bf16[768,2048]{1,0:T(8,128)(2,1)} fusion(bf16[128,768]{1,0:T(8,128)(2,1)S(1)} %copy-done.3, f32[128,2048]{1,0:T(8,128)S(1)} %get-tuple-element.12, f32[2048]{0:T(1024)S(1)} %copy-done.5, f32[128]{0:T(128)S(1)} %add_rsqrt_fusion), kind=kOutput, calls=%fused_computation | convolution fusion | flops 405012480 | bytes 4399616 | tf_op jit(solution)/shard_map/rs,rd->sd/dot_general | solution.py:222
  27.2 30.9 %all-to-all-start.1 = ((bf16[32,24,2048]{2,1,0:T(8,128)(2,1)}), bf16[32,24,2048]{2,1,0:T(8,128)(2,1)}, u32[]{:S(2)}, u32[]{:S(2)}) async-start(bf16[32,24,2048]{2,1,0:T(8,128)(2,1)} %bitcast.52), calls=%async_computation.1 | async-start | bytes 6291456 | tf_op jit(solution)/shard_map/all_to_all | solution.py:226
  58.2 0.5 compare_and_fusion
  58.7 70.9 %all-to-all-done.1 = bf16[32,24,2048]{2,1,0:T(8,128)(2,1)} async-done(((bf16[32,24,2048]{2,1,0:T(8,128)(2,1)}), bf16[32,24,2048]{2,1,0:T(8,128)(2,1)}, u32[]{:S(2)}, u32[]{:S(2)}) %all-to-all-start.1) | async-done | bytes 3145760 | tf_op jit(solution)/shard_map/all_to_all | solution.py:226
  129.6 2.9 %fusion.64 = (bf16[32,16,2048]{2,1,0:T(8,128)(2,1)S(1)}, bf16[32,16,2048]{2,1,0:T(8,128)(2,1)S(1)}) fusion(bf16[32,24,2048]{2,1,0:T(8,128)(2,1)} %all-to-all-done.1), kind=kLoop, calls=%fused_computation.79 | loop fusion | bytes 8388608 | tf_op jit(solution)/shard_map/slice | solution.py:232
  132.5 0.5 copy-done.8
  133.0 2.3 fusion.12
  135.3 2.2 fusion.7
  137.5 7.0 %convolution_convert_fusion.2 = bf16[512,2048]{1,0:T(8,128)(2,1)} fusion(bf16[2,512,2048]{2,1,0:T(8,128)(2,1)} %param.27, bf16[512,2048]{1,0:T(8,128)(2,1)} %bitcast.58, bf16[2,2048,512]{2,1,0:T(8,128)(2,1)} %param.26, f32[512,512]{1,0:T(8,128)} %fusion.12), kind=kOutput, calls=%fused_computation.3 | convolution fusion | flops 2150105088 | bytes 9437184 | tf_op jit(solution)/shard_map/dot_general | solution.py:236
  144.5 7.0 %convolution_convert_fusion.1 = bf16[512,2048]{1,0:T(8,128)(2,1)} fusion(bf16[2,512,2048]{2,1,0:T(8,128)(2,1)} %param.27, bf16[512,2048]{1,0:T(8,128)(2,1)} %bitcast.55, bf16[2,2048,512]{2,1,0:T(8,128)(2,1)} %param.26, f32[512,512]{1,0:T(8,128)} %fusion.7), kind=kOutput, calls=%fused_computation.2 | convolution fusion | flops 2150105088 | bytes 9437184 | tf_op jit(solution)/shard_map/dot_general | solution.py:236
  151.4 5.2 %select_select_fusion = bf16[32,24,2048]{2,1,0:T(8,128)(2,1)} fusion(bf16[32,16,2048]{2,1,0:T(8,128)(2,1)} %bitcast.56, bf16[32,16,2048]{2,1,0:T(8,128)(2,1)} %bitcast.53, pred[24]{0:T(512)(128)(4,1)} %get-tuple-element.14, pred[24]{0:T(512)(128)(4,1)S(1)} %get-tuple-element.13), kind=kLoop, calls=%fused_computation.1 | loop fusion | flops 3145728 | bytes 7340080 | tf_op jit(solution)/shard_map/jit(_where)/select_n | solution.py:239
  156.6 4.7 %all-to-all-start.2 = ((bf16[32,24,2048]{2,1,0:T(8,128)(2,1)}), bf16[32,24,2048]{2,1,0:T(8,128)(2,1)}, u32[]{:S(2)}, u32[]{:S(2)}) async-start(bf16[32,24,2048]{2,1,0:T(8,128)(2,1)} %select_select_fusion), calls=%async_computation.2 | async-start | bytes 6291456 | tf_op jit(solution)/shard_map/all_to_all | solution.py:240
  161.3 0.8 subtract_convert_fusion
  162.1 2.1 fusion.63
  164.2 68.7 %all-to-all-done.2 = bf16[32,24,2048]{2,1,0:T(8,128)(2,1)} async-done(((bf16[32,24,2048]{2,1,0:T(8,128)(2,1)}), bf16[32,24,2048]{2,1,0:T(8,128)(2,1)}, u32[]{:S(2)}, u32[]{:S(2)}) %all-to-all-start.2) | async-done | bytes 3145760 | tf_op jit(solution)/shard_map/all_to_all | solution.py:240
  232.9 4.4 %fusion.40 = f32[256,2048]{1,0:T(8,128)} fusion(bf16[768,2048]{1,0:T(8,128)(2,1)} %bitcast.15, bf16[128,768]{1,0:T(8,128)(2,1)} %get-tuple-element.7, bf16[128,768]{1,0:T(8,128)(2,1)} %get-tuple-element.8), kind=kOutput, calls=%fused_computation.43 | convolution fusion | flops 806092800 | bytes 5636096 | tf_op jit(solution)/shard_map/dot_general | solution.py:245
  237.3 4.5 %fusion.3 = bf16[128,2048]{1,0:T(8,128)(2,1)} fusion(f32[128,2048]{1,0:T(8,128)S(1)} %get-tuple-element.12, bf16[512,2048]{1,0:T(8,128)(2,1)} %param.24, bf16[2048,512]{1,0:T(8,128)(2,1)} %param.23, f32[256,2048]{1,0:T(8,128)} %fusion.40, f32[128,512]{1,0:T(8,128)S(1)} %fusion.63, f32[2048]{0:T(1024)S(1)} %copy-done.5, f32[128]{0:T(128)S(1)} %add_rsqrt_fusion), kind=kOutput, calls=%fused_computation.9 | convolution fusion | flops 539099136 | bytes 9183744 | tf_op jit(solution)/shard_map/dot_general | solution.py:277
  (17 shorter events, 0.1 us)
Async XLA Ops:
  0.0 22.7 %copy-start = (bf16[512,2048]{1,0:T(8,128)(2,1)S(1)}, bf16[512,2048]{1,0:T(8,128)(2,1)}, u32[]{:S(2)}) copy-start(bf16[512,2048]{1,0:T(8,128)(2,1)} %param.20) | copy-start | bytes 6291460
  0.0 18.9 %copy-start.6 = (s32[128,4]{0,1:T(4,128)S(1)}, s32[128,4]{0,1:T(4,128)}, u32[]{:S(2)}) copy-start(s32[128,4]{0,1:T(4,128)} %param.28) | copy-start | bytes 6148
  0.0 18.9 %copy-start.7 = (f32[128,4]{0,1:T(4,128)S(1)}, f32[128,4]{0,1:T(4,128)}, u32[]{:S(2)}) copy-start(f32[128,4]{0,1:T(4,128)} %param.29) | copy-start | bytes 6148
  14.2 7.9 %all-to-all-start = ((bf16[4,128,128]{1,2,0:T(8,128)(2,1)}), bf16[4,128,128]{1,2,0:T(8,128)(2,1)S(1)}, u32[]{:S(2)}, u32[]{:S(2)}) async-start(bf16[4,128,128]{1,2,0:T(8,128)(2,1)} %copy.38), calls=%async_computation | async-start | bytes 262144 | tf_op jit(solution)/shard_map/all_to_all | solution.py:267
  18.9 5.5 %copy-start.5 = (f32[2048]{0:T(1024)S(1)}, f32[2048]{0:T(1024)}, u32[]{:S(2)}) copy-start(f32[2048]{0:T(1024)} %param.21) | copy-start | bytes 24580
  22.1 0.7 copy-start.4
  22.7 1.7 copy-start.3
  27.2 102.4 %all-to-all-start.1 = ((bf16[32,24,2048]{2,1,0:T(8,128)(2,1)}), bf16[32,24,2048]{2,1,0:T(8,128)(2,1)}, u32[]{:S(2)}, u32[]{:S(2)}) async-start(bf16[32,24,2048]{2,1,0:T(8,128)(2,1)} %bitcast.52), calls=%async_computation.1 | async-start | bytes 6291456 | tf_op jit(solution)/shard_map/all_to_all | solution.py:226
  129.6 3.5 %copy-start.8 = (bf16[2,2048,512]{2,1,0:T(8,128)(2,1)S(1)}, bf16[2,2048,512]{2,1,0:T(8,128)(2,1)}, u32[]{:S(2)}) copy-start(bf16[2,2048,512]{2,1,0:T(8,128)(2,1)} %param.25) | copy-start | bytes 12582916
  132.5 2.8 %copy-start.2 = (bf16[32,16,2048]{2,1,0:T(8,128)(2,1)}, bf16[32,16,2048]{2,1,0:T(8,128)(2,1)S(1)}, u32[]{:S(2)}) copy-start(bf16[32,16,2048]{2,1,0:T(8,128)(2,1)S(1)} %get-tuple-element.9) | copy-start | bytes 6291460
  132.5 2.8 %copy-start.1 = (bf16[32,16,2048]{2,1,0:T(8,128)(2,1)}, bf16[32,16,2048]{2,1,0:T(8,128)(2,1)S(1)}, u32[]{:S(2)}) copy-start(bf16[32,16,2048]{2,1,0:T(8,128)(2,1)S(1)} %get-tuple-element.10) | copy-start | bytes 6291460
  156.6 76.3 %all-to-all-start.2 = ((bf16[32,24,2048]{2,1,0:T(8,128)(2,1)}), bf16[32,24,2048]{2,1,0:T(8,128)(2,1)}, u32[]{:S(2)}, u32[]{:S(2)}) async-start(bf16[32,24,2048]{2,1,0:T(8,128)(2,1)} %select_select_fusion), calls=%async_computation.2 | async-start | bytes 6291456 | tf_op jit(solution)/shard_map/all_to_all | solution.py:240
